TPU v7x, 32 devices: a whole 2x2x4 slice. The times are simulated.
32 devices in a mesh: sp: 8 (over z, y), tp: 4 (over x, core).
Axes of the slice: x: 2, y: 2, z: 4, core: 2. Of those that a mesh axis runs over, the one named last changes fastest.
Arguments:
- inputs: bfloat16 [4096, 4096], P('sp', 'tp'), may hold values from -24 to 24
- length: int32 [1], replicated, may hold values from 2049 to 4096
- win_query: bfloat16 [4096, 1536], P(None, 'tp'), may hold values from -8 to 8
- win_key: bfloat16 [4096, 512], P(None, 'tp'), may hold values from -8 to 8
- win_value: bfloat16 [4096, 512], P(None, 'tp'), may hold values from -1.5 to 1.5
- sink_logit: float32 [24], P('tp'), may hold values from 4 to 8
- diff_query: bfloat16 [4096, 1024], P(None, 'tp'), may hold values from -8 to 8
- diff_key: bfloat16 [4096, 1024], P(None, 'tp'), may hold values from -8 to 8
- diff_value: bfloat16 [4096, 1024], P(None, 'tp'), may hold values from -0.09375 to 0.09375
- mix_lambda: float32 [16], P('tp'), may hold values from 0.3 to 0.8
- head_gain: float32 [64], replicated, may hold values from 0.1 to 1.9
- win_out: bfloat16 [1536, 4096], P('tp'), may hold values from -0.125 to 0.125
- diff_out: bfloat16 [1024, 4096], P('tp'), may hold values from -0.125 to 0.125
Outputs:
- merged_out: bfloat16 [4096, 4096], P(('sp', 'tp'))
All inputs are finite; a program needn't handle non-finite values.
Results may differ from a plain program's by a relative error of at most 0.015.
Values may be sent and summed in bfloat16 or wider, within the bound.
No kernel may reach another device: no remote copies, remote signals or barrier semaphores. Data moves between devices by JAX's collectives and lax.ppermute only.
A program may use at most 128 MiB of HBM per device.

v0:
```python
import jax
import jax.numpy as jnp
from jax import lax
from jax.sharding import PartitionSpec as P

HEAD = 64
DQK = 32
GROUP = 3
WINDOW = 128
epsilon = 1e-06
masked_score = -1e30


def extended(block, sides, width):
    for axis, dim in sides:
        count = lax.axis_size(axis)
        forward = [(i, i + 1) for i in range(count - 1)]
        backward = [(target, source) for source, target in forward]
        low = lax.ppermute(
            lax.slice_in_dim(block, block.shape[dim] - width, None, axis=dim), axis, forward
        )
        high = lax.ppermute(lax.slice_in_dim(block, 0, width, axis=dim), axis, backward)
        block = jnp.concatenate([low, block, high], axis=dim)
    return block


def window_part(win_q, win_k, win_v, sink_logit, live_count, offset):
    row_count = win_q.shape[0]
    kv_local = win_k.shape[1] // HEAD
    stacked = jnp.stack(
        (win_k.reshape(row_count, kv_local, HEAD), win_v.reshape(row_count, kv_local, HEAD)), axis=2
    )
    stacked = stacked.reshape(row_count, kv_local * 2 * HEAD)
    padded = extended(stacked, (("sp", 0),), WINDOW)
    padded = padded.reshape(row_count + 2 * WINDOW, kv_local, 2, HEAD)
    keys_win = padded[:, :, 0]
    values_win = padded[:, :, 1]
    queries = win_q.reshape(row_count, kv_local, GROUP, HEAD)
    sink_table = sink_logit.reshape(kv_local, GROUP)
    query_pos = offset + jnp.arange(row_count, dtype=jnp.int32)
    key_pos = offset - WINDOW + jnp.arange(row_count + 2 * WINDOW, dtype=jnp.int32)
    allowed = (
        (jnp.abs(query_pos[:, None] - key_pos[None, :]) <= WINDOW)
        & (key_pos[None, :] >= 0)
        & (key_pos[None, :] < live_count)
    )
    scores = jnp.einsum(
        "qhgd,khd->hgqk", queries, keys_win, preferred_element_type=jnp.float32
    ) * HEAD ** (-0.5)
    scores = jnp.where(allowed[None, None], scores, masked_score)
    row_max = jnp.maximum(jnp.max(scores, axis=-1), sink_table[:, :, None])
    exponent = jnp.where(allowed[None, None], jnp.exp(scores - row_max[..., None]), 0.0)
    denominator = jnp.sum(exponent, axis=-1) + jnp.exp(sink_table[:, :, None] - row_max)
    result = jnp.einsum(
        "hgqk,khd->qhgd",
        exponent.astype(jnp.bfloat16),
        values_win,
        preferred_element_type=jnp.float32,
    )
    result = result / jnp.transpose(denominator, (2, 0, 1))[..., None]
    result = jnp.where((query_pos < live_count)[:, None, None, None], result, 0.0)
    return result.reshape(row_count, kv_local * GROUP * HEAD).astype(jnp.bfloat16)


def attend(running, queries, key_part, value_part, live_count, block_total, query_step):
    key_length = key_part.shape[0]
    key_step = 4096

    def one_query_block(block_index, block_state):
        running_max, total_sum, weighted = block_state
        row_begin = block_index * query_step
        query_slab = lax.dynamic_slice_in_dim(queries, row_begin, query_step, 0)
        start_state = (
            lax.dynamic_slice_in_dim(running_max, row_begin, query_step, 2),
            lax.dynamic_slice_in_dim(total_sum, row_begin, query_step, 2),
            lax.dynamic_slice_in_dim(weighted, row_begin, query_step, 2),
        )

        def one_key_block(key_index, key_state):
            block_max, block_sum, block_weighted = key_state
            key_begin = key_index * key_step
            key_slab = lax.dynamic_slice_in_dim(key_part, key_begin, key_step, 0)
            value_slab = lax.dynamic_slice_in_dim(value_part, key_begin, key_step, 0)
            key_pos = key_begin + jnp.arange(key_step, dtype=jnp.int32)
            allowed = key_pos < live_count
            scores = jnp.einsum(
                "qhmd,khmd->hmqk", query_slab, key_slab, preferred_element_type=jnp.float32
            ) * DQK ** (-0.5)
            scores = jnp.where(allowed, scores, masked_score)
            new_max = jnp.maximum(block_max, jnp.max(scores, axis=-1))
            rescale = jnp.exp(block_max - new_max)
            exponent = jnp.where(allowed, jnp.exp(scores - new_max[..., None]), 0.0)
            new_total = block_sum * rescale + jnp.sum(exponent, axis=-1)
            new_weighted = block_weighted * rescale[..., None] + jnp.einsum(
                "hmqk,khd->hmqd",
                exponent.astype(jnp.bfloat16),
                value_slab,
                preferred_element_type=jnp.float32,
            )
            return (new_max, new_total, new_weighted)

        final_state = lax.fori_loop(0, key_length // key_step, one_key_block, start_state)
        return (
            lax.dynamic_update_slice_in_dim(running_max, final_state[0], row_begin, 2),
            lax.dynamic_update_slice_in_dim(total_sum, final_state[1], row_begin, 2),
            lax.dynamic_update_slice_in_dim(weighted, final_state[2], row_begin, 2),
        )

    return lax.fori_loop(0, block_total, one_query_block, running)


def diff_part(diff_q, diff_k, diff_v, mix_lambda, head_gain, live_count, offset):
    row_count = diff_q.shape[0]
    heads_local = mix_lambda.shape[0]
    query_step = 128
    positions = offset + jnp.arange(row_count, dtype=jnp.int32)
    live_rows = jnp.sum((positions < live_count).astype(jnp.int32))
    block_total = (live_rows + query_step - 1) // query_step
    queries = diff_q.reshape(row_count, heads_local, 2, DQK)
    zero_state = (
        jnp.full((heads_local, 2, row_count), masked_score, jnp.float32),
        jnp.zeros((heads_local, 2, row_count), jnp.float32),
        jnp.zeros((heads_local, 2, row_count, HEAD), jnp.float32),
    )
    key_part = lax.all_gather(diff_k, "sp", axis=0, tiled=True).reshape(-1, heads_local, 2, DQK)
    value_part = lax.all_gather(diff_v, "sp", axis=0, tiled=True).reshape(-1, heads_local, HEAD)
    running = lax.cond(
        jnp.int32(0) < live_count,
        lambda inner_state: attend(
            inner_state, queries, key_part, value_part, live_count, block_total, query_step
        ),
        lambda inner_state: inner_state,
        zero_state,
    )
    total_sum = running[1]
    safe_total = jnp.where(total_sum > 0.0, total_sum, 1.0)
    map_rows = running[2] / safe_total[..., None]
    mixed_rows = map_rows[:, 0] - mix_lambda[:, None, None] * map_rows[:, 1]
    normed = (
        mixed_rows
        * lax.rsqrt(jnp.mean(mixed_rows * mixed_rows, axis=-1, keepdims=True) + epsilon)
        * head_gain
    )
    normed = jnp.where((positions < live_count)[None, :, None], normed, 0.0)
    result = (
        jnp.transpose(normed, (1, 0, 2)).reshape(row_count, heads_local * HEAD).astype(jnp.bfloat16)
    )
    return result


def body(
    inputs,
    length,
    win_query,
    win_key,
    win_value,
    sink_logit,
    diff_query,
    diff_key,
    diff_value,
    mix_lambda,
    head_gain,
    win_out,
    diff_out,
):
    row_count = inputs.shape[0]
    live_count = length[0]
    weights = (win_query, win_key, win_value, diff_query, diff_key, diff_value)
    segment = lax.all_gather(inputs, "tp", axis=1, tiled=True)
    summed = tuple(
        (jnp.dot(segment, weight, preferred_element_type=jnp.float32) for weight in weights)
    )
    win_q, win_k, win_v, diff_q, diff_k, diff_v = [total.astype(jnp.bfloat16) for total in summed]
    offset = lax.axis_index("sp") * row_count
    win_rows = window_part(win_q, win_k, win_v, sink_logit, live_count, offset)
    diff_rows = diff_part(diff_q, diff_k, diff_v, mix_lambda, head_gain, live_count, offset)
    partial_value = jnp.dot(win_rows, win_out, preferred_element_type=jnp.float32)
    return lax.psum_scatter(
        (partial_value + jnp.dot(diff_rows, diff_out, preferred_element_type=jnp.float32)).astype(
            jnp.bfloat16
        ),
        "tp",
        scatter_dimension=0,
        tiled=True,
    )


def solution(mesh):
    placed = (
        P("sp", "tp"),
        P(),
        P(None, "tp"),
        P(None, "tp"),
        P(None, "tp"),
        P("tp"),
        P(None, "tp"),
        P(None, "tp"),
        P(None, "tp"),
        P("tp"),
        P(),
        P("tp", None),
        P("tp", None),
    )
    return jax.shard_map(
        body, mesh=mesh, in_specs=placed, out_specs=P(("sp", "tp"), None), check_vma=False
    )
```

profile of v0, /device:TPU:0, one launch (start us, length us, event | category | flops | bytes accessed | tf_op | source)
XLA Modules:
  0.0 299.4 jit_solution(1611999572940378291)
XLA Ops:
  6.5 0.7 all-gather.4.cloned.1.call-update
  7.3 38.8 %all-gather.4.cloned.1.call-done = bf16[512,4096]{1,0:T(8,128)(2,1)} async-done(((bf16[512,1024]{1,0:T(8,128)(2,1)}), bf16[512,4096]{1,0:T(8,128)(2,1)}) %all-gather.4.cloned.1.call-update) | async-done | bytes 4194320 | tf_op jit(solution)/shard_map/all_gather | solution.py:169
  46.1 4.8 %convolution_convert_fusion.1 = bf16[512,256]{1,0:T(8,128)(2,1)} fusion(bf16[512,4096]{1,0:T(8,128)(2,1)} %all-gather.4.cloned.1.call-done, bf16[4096,256]{1,0:T(8,128)(2,1)} %param.25), kind=kOutput, calls=%fused_computation.34 | convolution fusion | flops 1073872896 | bytes 6553600 | tf_op jit(solution)/shard_map/dot_general | solution.py:171
  51.8 0.8 fusion.30
  52.6 4.4 %convolution_convert_fusion.4 = bf16[512,128]{0,1:T(8,128)(2,1)S(1)} fusion(bf16[512,4096]{1,0:T(8,128)(2,1)} %all-gather.4.cloned.1.call-done, bf16[4096,128]{1,0:T(8,128)(2,1)} %param.21), kind=kOutput, calls=%fused_computation.37 | convolution fusion | flops 536936448 | bytes 5373952 | tf_op jit(solution)/shard_map/dot_general | solution.py:171
  57.0 1.5 convolution_convert_fusion.5
  60.5 1.3 collective-permute-start.1
  61.8 5.2 %collective-permute-start = (bf16[128,256]{0,1:T(8,128)(2,1)}, bf16[128,256]{0,1:T(8,128)(2,1)}, u32[]{:S(2)}, u32[]{:S(2)}) collective-permute-start(bf16[128,256]{0,1:T(8,128)(2,1)} %bitcast.8), channel_id=1, source_target_pairs={{0,4},{4,8},{8,12},{12,16},{16,20},{20,24},{24,28},{1,5},{5,9},{9,... | collective-permute-start | bytes 196616 | tf_op jit(solution)/shard_map/ppermute | solution.py:19
  67.0 2.0 convolution_convert_fusion.2
  69.2 5.2 %convolution_convert_fusion = bf16[512,384]{0,1:T(8,128)(2,1)S(1)} fusion(bf16[512,4096]{1,0:T(8,128)(2,1)} %all-gather.4.cloned.1.call-done, bf16[4096,384]{1,0:T(8,128)(2,1)} %param.19), kind=kOutput, calls=%fused_computation.33 | convolution fusion | flops 1610809344 | bytes 7733248 | tf_op jit(solution)/shard_map/dot_general | solution.py:171
  74.4 2.0 convolution_convert_fusion.3
  76.4 0.9 pad_maximum_fusion
  77.3 1.7 fusion.23
  79.1 2.3 fusion.24
  81.4 2.7 fusion.40
  84.1 5.6 %fusion.52 = f32[512,4096]{1,0:T(8,128)} fusion(bf16[512,384]{0,1:T(8,128)(2,1)S(1)} %bitcast.123, bf16[384,4096]{1,0:T(8,128)(2,1)S(1)} %copy-done), kind=kOutput, calls=%fused_computation.68 | convolution fusion | flops 1610612736 | bytes 11927552 | tf_op jit(solution)/shard_map/dot_general | solution.py:177
  89.7 11.3 %all-gather.8.cloned.1.call-done = bf16[4096,256]{1,0:T(8,128)(2,1)} async-done(((bf16[512,256]{1,0:T(8,128)(2,1)}), bf16[4096,256]{1,0:T(8,128)(2,1)}) %all-gather.8.cloned.1.call-update) | async-done | bytes 2097168 | tf_op jit(solution)/shard_map/all_gather | solution.py:126
  101.0 49.8 %all-gather.6.cloned.1.call-done = bf16[4096,256]{1,0:T(8,128)(2,1)} async-done(((bf16[512,256]{1,0:T(8,128)(2,1)}), bf16[4096,256]{1,0:T(8,128)(2,1)}) %all-gather.6.cloned.1.call-update) | async-done | bytes 2097168 | tf_op jit(solution)/shard_map/all_gather | solution.py:125
  150.8 89.2 %conditional.1 = (f32[4,2,512]{2,1,0:T(2,128)}, f32[4,2,512,64]{2,3,1,0:T(8,128)}) conditional(s32[]{:T(128)} %convert_element_type.55, () %tuple.34, (s32[512]{0:T(512)S(1)}, bf16[512,256]{1,0:T(8,128)(2,1)S(1)}, bf16[4096,256]{1,0:T(8,128)(2,1)}, bf16[4096,256]{1,0:T(8,128)(2,1)}, s32[]{:T(128)}, /*index=5*/s32[]{:T(128)}) %tuple.79), branch_computations={%region_3.4_spmd, %region_4.9_spmd.clone} | conditional | flops 859970048 | bytes 132364824 | solution.py:127
  152.3 4.1 %copy.34 = bf16[4096,256]{0,1:T(8,128)(2,1)} copy(bf16[4096,256]{1,0:T(8,128)(2,1)} %get-tuple-element.250) | data formatting | bytes 4194304 | tf_op jit(solution)/shard_map
  156.4 2.9 copy.33
  159.9 1.1 broadcast_in_dim.105
  161.0 79.0 %while.37 = (s32[]{:T(128)}, f32[4,2,512]{2,1,0:T(2,128)S(1)}, f32[4,2,512]{2,1,0:T(2,128)}, f32[4,2,512,64]{2,3,1,0:T(8,128)}, s32[]{:T(128)}, /*index=5*/s32[]...) while((s32[]{:T(128)}, f32[4,2,512]{2,1,0:T(2,128)S(1)}, ...), condition=%wide.region_8.8_spmd, body=%wide.region_5.7_spmd.sunk | while | flops 859969536 | bytes 122368224 | solution.py:109
  161.7 2.7 fusion.82
  164.5 4.9 %fusion.83 = f32[4,2,128]{2,1,0:T(2,128)S(1)} fusion(f32[4,2,128,4096]{3,2,1,0:T(8,128)S(1)} %get-tuple-element.357, f32[4,2,128]{2,1,0:T(2,128)S(1)} %get-tuple-element.358, pred[4096]{0:T(1024)(128)(4,1)S(1)} %iota_compare_fusion.2), kind=kLoop, calls=%fused_computation.4.clone.1 | loop fusion | flops 20970496 | bytes 16789504 | tf_op jit(solution)/shard_map/cond/branch_1_fun/while/body/while/body/eval_jaxpr/reduce_sum | solution.py:93
  169.4 0.8 copy-done.2
  170.2 1.3 add_dynamic-update-slice_fusion.2
  171.5 9.3 %fusion.84 = f32[4,2,512,64]{2,3,1,0:T(8,128)} fusion(f32[4,2,512,64]{2,3,1,0:T(8,128)} %get-tuple-element.377, s32[]{:T(128)S(6)} %select_n.128, bf16[4096,4,64]{0,2,1:T(8,128)(2,1)} %get-tuple-element.395, f32[4,2,128,4096]{3,2,1,0:T(8,128)} %copy-done.2, f32[4,2,128]{2,1,0:T(2,128)S(1)} %get-tuple-element.358, ...), kind=kOutput, calls=%fused_computation.9.clone.1 | convolution fusion | flops 557973504 | bytes 19410948 | tf_op jit(solution)/shard_map/cond/branch_1_fun/while/body/while/body/eval_jaxpr/hmqk,khd->hmqd/dot_general | solution.py:94
  181.5 2.7 fusion.82
  184.2 4.9 %fusion.83 = f32[4,2,128]{2,1,0:T(2,128)S(1)} fusion(f32[4,2,128,4096]{3,2,1,0:T(8,128)S(1)} %get-tuple-element.357, f32[4,2,128]{2,1,0:T(2,128)S(1)} %get-tuple-element.358, pred[4096]{0:T(1024)(128)(4,1)S(1)} %iota_compare_fusion.2), kind=kLoop, calls=%fused_computation.4.clone.1 | loop fusion | flops 20970496 | bytes 16789504 | tf_op jit(solution)/shard_map/cond/branch_1_fun/while/body/while/body/eval_jaxpr/reduce_sum | solution.py:93
  189.1 0.8 copy-done.2
  190.0 1.3 add_dynamic-update-slice_fusion.2
  191.2 9.3 %fusion.84 = f32[4,2,512,64]{2,3,1,0:T(8,128)} fusion(f32[4,2,512,64]{2,3,1,0:T(8,128)} %get-tuple-element.377, s32[]{:T(128)S(6)} %select_n.128, bf16[4096,4,64]{0,2,1:T(8,128)(2,1)} %get-tuple-element.395, f32[4,2,128,4096]{3,2,1,0:T(8,128)} %copy-done.2, f32[4,2,128]{2,1,0:T(2,128)S(1)} %get-tuple-element.358, ...), kind=kOutput, calls=%fused_computation.9.clone.1 | convolution fusion | flops 557973504 | bytes 19410948 | tf_op jit(solution)/shard_map/cond/branch_1_fun/while/body/while/body/eval_jaxpr/hmqk,khd->hmqd/dot_general | solution.py:94
  200.6 0.7 iota_compare_fusion.2
  201.2 2.7 fusion.82
  204.0 4.9 %fusion.83 = f32[4,2,128]{2,1,0:T(2,128)S(1)} fusion(f32[4,2,128,4096]{3,2,1,0:T(8,128)S(1)} %get-tuple-element.357, f32[4,2,128]{2,1,0:T(2,128)S(1)} %get-tuple-element.358, pred[4096]{0:T(1024)(128)(4,1)S(1)} %iota_compare_fusion.2), kind=kLoop, calls=%fused_computation.4.clone.1 | loop fusion | flops 20970496 | bytes 16789504 | tf_op jit(solution)/shard_map/cond/branch_1_fun/while/body/while/body/eval_jaxpr/reduce_sum | solution.py:93
  208.9 0.8 copy-done.2
  209.7 1.3 add_dynamic-update-slice_fusion.2
  211.0 9.3 %fusion.84 = f32[4,2,512,64]{2,3,1,0:T(8,128)} fusion(f32[4,2,512,64]{2,3,1,0:T(8,128)} %get-tuple-element.377, s32[]{:T(128)S(6)} %select_n.128, bf16[4096,4,64]{0,2,1:T(8,128)(2,1)} %get-tuple-element.395, f32[4,2,128,4096]{3,2,1,0:T(8,128)} %copy-done.2, f32[4,2,128]{2,1,0:T(2,128)S(1)} %get-tuple-element.358, ...), kind=kOutput, calls=%fused_computation.9.clone.1 | convolution fusion | flops 557973504 | bytes 19410948 | tf_op jit(solution)/shard_map/cond/branch_1_fun/while/body/while/body/eval_jaxpr/hmqk,khd->hmqd/dot_general | solution.py:94
  221.0 2.7 fusion.82
  223.7 4.9 %fusion.83 = f32[4,2,128]{2,1,0:T(2,128)S(1)} fusion(f32[4,2,128,4096]{3,2,1,0:T(8,128)S(1)} %get-tuple-element.357, f32[4,2,128]{2,1,0:T(2,128)S(1)} %get-tuple-element.358, pred[4096]{0:T(1024)(128)(4,1)S(1)} %iota_compare_fusion.2), kind=kLoop, calls=%fused_computation.4.clone.1 | loop fusion | flops 20970496 | bytes 16789504 | tf_op jit(solution)/shard_map/cond/branch_1_fun/while/body/while/body/eval_jaxpr/reduce_sum | solution.py:93
  228.6 0.8 copy-done.2
  229.5 1.3 add_dynamic-update-slice_fusion.2
  230.7 9.3 %fusion.84 = f32[4,2,512,64]{2,3,1,0:T(8,128)} fusion(f32[4,2,512,64]{2,3,1,0:T(8,128)} %get-tuple-element.377, s32[]{:T(128)S(6)} %select_n.128, bf16[4096,4,64]{0,2,1:T(8,128)(2,1)} %get-tuple-element.395, f32[4,2,128,4096]{3,2,1,0:T(8,128)} %copy-done.2, f32[4,2,128]{2,1,0:T(2,128)S(1)} %get-tuple-element.358, ...), kind=kOutput, calls=%fused_computation.9.clone.1 | convolution fusion | flops 557973504 | bytes 19410948 | tf_op jit(solution)/shard_map/cond/branch_1_fun/while/body/while/body/eval_jaxpr/hmqk,khd->hmqd/dot_general | solution.py:94
  240.1 0.9 compare_select_fusion
  240.9 1.4 broadcast_divide_fusion
  242.7 6.8 %add_convert_fusion = bf16[512,4096]{1,0:T(8,128)(2,1)} fusion(f32[512,4096]{1,0:T(8,128)} %fusion.52, bf16[512,256]{0,1:T(8,128)(2,1)S(1)} %bitcast.122, bf16[256,4096]{1,0:T(8,128)(2,1)S(1)} %copy-done.5), kind=kOutput, calls=%fused_computation.23 | convolution fusion | flops 1077936128 | bytes 14942208 | tf_op jit(solution)/shard_map/dot_general | solution.py:179
  249.6 43.2 %reduce-scatter.2.cloned.1.call-done = bf16[128,4096]{1,0:T(8,128)(2,1)} async-done(((bf16[512,4096]{1,0:T(8,128)(2,1)}), bf16[128,4096]{1,0:T(8,128)(2,1)}) %reduce-scatter.2.cloned.1.call-update) | async-done | bytes 1048592 | tf_op jit(solution)/shard_map/reduce_scatter | solution.py:178
  (77 shorter events, 6.4 us)
Async XLA Ops:
  6.5 77.6 %copy-start = (bf16[384,4096]{1,0:T(8,128)(2,1)S(1)}, bf16[384,4096]{1,0:T(8,128)(2,1)}, u32[]{:S(2)}) copy-start(bf16[384,4096]{1,0:T(8,128)(2,1)} %param.28) | copy-start | bytes 9437188
  6.5 39.6 %all-gather.4.cloned.1.call-start = ((), (), s32[]{:S(2)}) async-start(), calls=%async_computation.1 | async-start | bytes 5242880 | tf_op jit(solution)/shard_map/all_gather | solution.py:169
  7.3 44.4 %copy-start.16 = (f32[6]{0:T(128)S(1)}, f32[6]{0:T(128)}, u32[]{:S(2)}) copy-start(f32[6]{0:T(128)} %param.22) | copy-start | bytes 76
  7.3 93.7 %all-gather.8.cloned.1.call-start = ((), (), s32[]{:S(2)}) async-start(), calls=%async_computation.3 | async-start | bytes 2359296 | tf_op jit(solution)/shard_map/all_gather | solution.py:126
  51.0 99.8 %all-gather.6.cloned.1.call-start = ((), (), s32[]{:S(2)}) async-start(), calls=%async_computation.2 | async-start | bytes 2359296 | tf_op jit(solution)/shard_map/all_gather | solution.py:125
  51.8 5.2 %copy-start.3 = (bf16[512,4096]{1,0:T(8,128)(2,1)S(1)}, bf16[512,4096]{1,0:T(8,128)(2,1)}, u32[]{:S(2)}) copy-start(bf16[512,4096]{1,0:T(8,128)(2,1)} %all-gather.4.cloned.1.call-done) | copy-start | bytes 12582916
  51.8 5.2 %copy-start.10 = (bf16[4096,128]{1,0:T(8,128)(2,1)S(1)}, bf16[4096,128]{1,0:T(8,128)(2,1)}, u32[]{:S(2)}) copy-start(bf16[4096,128]{1,0:T(8,128)(2,1)} %param.20) | copy-start | bytes 3145732
  57.0 1.5 copy-start.6
  57.0 9.9 %copy-start.14 = (bf16[4096,256]{1,0:T(8,128)(2,1)S(1)}, bf16[4096,256]{1,0:T(8,128)(2,1)}, u32[]{:S(2)}) copy-start(bf16[4096,256]{1,0:T(8,128)(2,1)} %param.24) | copy-start | bytes 6291460
  58.6 0.7 copy-start.8
  60.5 15.9 %collective-permute-start.1 = (bf16[128,256]{0,1:T(8,128)(2,1)}, bf16[128,256]{0,1:T(8,128)(2,1)}, u32[]{:S(2)}, u32[]{:S(2)}) collective-permute-start(bf16[128,256]{0,1:T(8,128)(2,1)} %bitcast.10), channel_id=1, source_target_pairs={{4,0},{8,4},{12,8},{16,12},{20,16},{24,20},{28,24},{5,1},{9,5},{13... | collective-permute-start | bytes 196616 | tf_op jit(solution)/shard_map/ppermute | solution.py:22
  61.8 14.6 %collective-permute-start = (bf16[128,256]{0,1:T(8,128)(2,1)}, bf16[128,256]{0,1:T(8,128)(2,1)}, u32[]{:S(2)}, u32[]{:S(2)}) collective-permute-start(bf16[128,256]{0,1:T(8,128)(2,1)} %bitcast.8), channel_id=1, source_target_pairs={{0,4},{4,8},{8,12},{12,16},{16,20},{20,24},{24,28},{1,5},{5,9},{9,... | collective-permute-start | bytes 196616 | tf_op jit(solution)/shard_map/ppermute | solution.py:19
  69.0 223.9 %reduce-scatter.2.cloned.1.call-start = ((), (), s32[]{:S(2)}) async-start(), calls=%async_computation.4 | async-start | bytes 5242880 | tf_op jit(solution)/shard_map/reduce_scatter | solution.py:178
  69.2 5.2 %copy-start.4 = (bf16[512,4096]{1,0:T(8,128)(2,1)S(1)}, bf16[512,4096]{1,0:T(8,128)(2,1)}, u32[]{:S(2)}) copy-start(bf16[512,4096]{1,0:T(8,128)(2,1)} %all-gather.4.cloned.1.call-done) | copy-start | bytes 12582916
  69.2 5.2 %copy-start.15 = (bf16[4096,256]{1,0:T(8,128)(2,1)S(1)}, bf16[4096,256]{1,0:T(8,128)(2,1)}, u32[]{:S(2)}) copy-start(bf16[4096,256]{1,0:T(8,128)(2,1)} %param.23) | copy-start | bytes 6291460
  74.4 2.0 copy-start.7
  74.4 2.0 copy-start.9
  84.1 66.7 %copy-start.11 = (bf16[512,256]{1,0:T(8,128)(2,1)S(1)}, bf16[512,256]{1,0:T(8,128)(2,1)}, u32[]{:S(2)}) copy-start(bf16[512,256]{1,0:T(8,128)(2,1)} %convolution_convert_fusion.3) | copy-start | bytes 786436
  150.8 91.5 %copy-start.12 = (f32[4]{0:T(128)S(1)}, f32[4]{0:T(128)}, u32[]{:S(2)}) copy-start(f32[4]{0:T(128)} %param.26) | copy-start | bytes 52
  150.8 91.7 %copy-start.13 = (f32[64]{0:T(128)S(1)}, f32[64]{0:T(128)}, u32[]{:S(2)}) copy-start(f32[64]{0:T(128)} %param.27) | copy-start | bytes 772
  164.4 5.7 %copy-start.2 = (f32[4,2,128,4096]{3,2,1,0:T(8,128)}, f32[4,2,128,4096]{3,2,1,0:T(8,128)S(1)}, u32[]{:S(2)}) copy-start(f32[4,2,128,4096]{3,2,1,0:T(8,128)S(1)} %get-tuple-element.357) | copy-start | bytes 50331652 | tf_op jit(solution)/shard_map/cond/branch_1_fun/while
  184.2 5.7 %copy-start.2 = (f32[4,2,128,4096]{3,2,1,0:T(8,128)}, f32[4,2,128,4096]{3,2,1,0:T(8,128)S(1)}, u32[]{:S(2)}) copy-start(f32[4,2,128,4096]{3,2,1,0:T(8,128)S(1)} %get-tuple-element.357) | copy-start | bytes 50331652 | tf_op jit(solution)/shard_map/cond/branch_1_fun/while
  204.0 5.7 %copy-start.2 = (f32[4,2,128,4096]{3,2,1,0:T(8,128)}, f32[4,2,128,4096]{3,2,1,0:T(8,128)S(1)}, u32[]{:S(2)}) copy-start(f32[4,2,128,4096]{3,2,1,0:T(8,128)S(1)} %get-tuple-element.357) | copy-start | bytes 50331652 | tf_op jit(solution)/shard_map/cond/branch_1_fun/while
  223.7 5.7 %copy-start.2 = (f32[4,2,128,4096]{3,2,1,0:T(8,128)}, f32[4,2,128,4096]{3,2,1,0:T(8,128)S(1)}, u32[]{:S(2)}) copy-start(f32[4,2,128,4096]{3,2,1,0:T(8,128)S(1)} %get-tuple-element.357) | copy-start | bytes 50331652 | tf_op jit(solution)/shard_map/cond/branch_1_fun/while
  240.1 2.7 copy-start.5
  242.7 50.1 %copy-start.1 = (bf16[384,4096]{1,0:T(8,128)(2,1)S(1)}, bf16[384,4096]{1,0:T(8,128)(2,1)}, u32[]{:S(2)}) copy-start(bf16[384,4096]{1,0:T(8,128)(2,1)} %param.28) | copy-start | bytes 9437188
Sparse Core Ops, SparseCore 0:
  8.9 37.1 all-gather.3
  51.1 49.8 all-gather.7
  103.1 47.6 all-gather.5
  249.7 43.0 reduce-scatter.1
where the time goes:
time: 300 us; the launch traced here: 299 us
  waiting for transfers between devices  144 us (48%)
  matrix products  84.8 us (28%)
  other arithmetic  34.7 us (12%)
  local copies, waits for them, and re-layouts  14.3 us (5%)
  between operations  14.1 us (5%)
  starting transfers between devices  6.77 us (2%)
    all_gather x1, waiting for transfers between devices, diff_part(): lax.all_gather(diff_k, 'sp', axis=0, tiled=True)  49.8 us
    reduce_scatter x1, waiting for transfers between devices, body(): lax.psum_scatter((partial_value + jnp.dot(diff_rows, diff_out, preferred_...  43.2 us
    all_gather x1, waiting for transfers between devices, body(): segment = lax.all_gather(inputs, 'tp', axis=1, tiled=True)  38.8 us
    dot_general x4, matrix products, one_key_block(): jnp.einsum('hmqk,khd->hmqd', exponent.astype(jnp.bfloat16), value_slab, p...  37.3 us
    dot_general x6, matrix products, body(): jnp.dot(segment, weight, preferred_element_type=jnp.float32)  19.8 us
    reduce_sum x4, other arithmetic, one_key_block(): new_total = block_sum * rescale + jnp.sum(exponent, axis=-1)  19.5 us
    all_gather x1, waiting for transfers between devices, diff_part(): lax.all_gather(diff_v, 'sp', axis=0, tiled=True)  11.3 us
    dot_general x4, matrix products, one_key_block(): jnp.einsum('qhmd,khmd->hmqk', query_slab, key_slab, preferred_element_typ...  11 us
  transfers between devices with their start and end apart: 6, of which 4 were waited for; matrix products, arithmetic and copies ran while one was open for 10% of the time, Pallas kernels for 0%

commit v1 on v0

--- a/solution.py
+++ b/solution.py
@@ -166,7 +166,8 @@
     row_count = inputs.shape[0]
     live_count = length[0]
     weights = (win_query, win_key, win_value, diff_query, diff_key, diff_value)
-    segment = lax.all_gather(inputs, "tp", axis=1, tiled=True)
+    switch_yards = lambda packet: jnp.concatenate(lax.all_gather(packet, axis_name="tp"), 1)
+    segment = switch_yards(inputs)
     summed = tuple(
         (jnp.dot(segment, weight, preferred_element_type=jnp.float32) for weight in weights)
     )

time: 300 us -> 306 us (1.020)
  local copies, waits for them, and re-layouts: 14.3 us -> 20.5 us
    reshape x0 -> x1, local copies, waits for them, and re-layouts: none -> 6.2 us  [body(): jnp.concatenate(lax.all_gather(packet, axis_name='tp'), 1)]
  transfers between devices with their start and end apart: 6 -> 6, of which waited for: 4 -> 4; matrix products, arithmetic and copies ran while one was open for 10% -> 11% of each run, Pallas kernels for 0% -> 0%
where the time goes in v1:
time: 306 us
  waiting for transfers between devices  142 us (46%)
  matrix products  87.1 us (28%)
  other arithmetic  34.6 us (11%)
  local copies, waits for them, and re-layouts  20.5 us (7%)
  between operations  14 us (5%)
  starting transfers between devices  6.75 us (2%)
    all_gather x1, waiting for transfers between devices, diff_part(): lax.all_gather(diff_k, 'sp', axis=0, tiled=True)  49.8 us
    reduce_scatter x1, waiting for transfers between devices, body(): lax.psum_scatter((partial_value + jnp.dot(diff_rows, diff_out, preferred_...  43.2 us
    all_gather x1, waiting for transfers between devices, body(): lax.all_gather(packet, axis_name='tp')  38.8 us
    dot_general x4, matrix products, one_key_block(): jnp.einsum('hmqk,khd->hmqd', exponent.astype(jnp.bfloat16), value_slab, p...  37.3 us
    dot_general x6, matrix products, body(): jnp.dot(segment, weight, preferred_element_type=jnp.float32)  22.1 us
    reduce_sum x4, other arithmetic, one_key_block(): new_total = block_sum * rescale + jnp.sum(exponent, axis=-1)  19.5 us
    dot_general x4, matrix products, one_key_block(): jnp.einsum('qhmd,khmd->hmqk', query_slab, key_slab, preferred_element_typ...  11 us
    all_gather x1, waiting for transfers between devices, diff_part(): lax.all_gather(diff_v, 'sp', axis=0, tiled=True)  9.35 us
  transfers between devices with their start and end apart: 6, of which 4 were waited for; matrix products, arithmetic and copies ran while one was open for 11% of the time, Pallas kernels for 0%

profile of v1, /device:TPU:0, one launch (start us, length us, event | category | flops | bytes accessed | tf_op | source)
XLA Modules:
  0.0 305.7 jit_solution(2350559141903219995)
XLA Ops:
  6.5 0.7 all-gather.9.cloned.1.call-update
  7.3 38.8 %all-gather.9.cloned.1.call-done = bf16[2048,1024]{1,0:T(8,128)(2,1)} async-done(((bf16[512,1024]{1,0:T(8,128)(2,1)}), bf16[2048,1024]{1,0:T(8,128)(2,1)}) %all-gather.9.cloned.1.call-update) | async-done | bytes 4194320 | tf_op jit(solution)/shard_map/all_gather | solution.py:169
  46.1 6.2 %copy.28 = bf16[512,4,1024]{0,2,1:T(8,128)(2,1)} copy(bf16[512,4,1024]{2,0,1:T(8,128)(2,1)} %bitcast.126) | data formatting | bytes 8388608 | tf_op jit(solution)/shard_map/reshape | solution.py:169
  52.3 4.9 %convolution_convert_fusion.1 = bf16[512,256]{1,0:T(8,128)(2,1)} fusion(bf16[512,4096]{0,1:T(8,128)(2,1)} %bitcast.120, bf16[4096,256]{1,0:T(8,128)(2,1)} %param.25), kind=kOutput, calls=%fused_computation.34 | convolution fusion | flops 1073872896 | bytes 6553600 | tf_op jit(solution)/shard_map/dot_general | solution.py:172
  58.1 0.8 fusion.30
  58.8 3.7 %convolution_convert_fusion.4 = bf16[512,128]{0,1:T(8,128)(2,1)S(1)} fusion(bf16[512,4096]{0,1:T(8,128)(2,1)} %bitcast.121, bf16[4096,128]{1,0:T(8,128)(2,1)} %param.21), kind=kOutput, calls=%fused_computation.37 | convolution fusion | flops 536936448 | bytes 5373952 | tf_op jit(solution)/shard_map/dot_general | solution.py:172
  62.6 0.8 convolution_convert_fusion.5
  65.3 1.3 collective-permute-start.1
  66.6 5.2 %collective-permute-start = (bf16[128,256]{0,1:T(8,128)(2,1)}, bf16[128,256]{0,1:T(8,128)(2,1)}, u32[]{:S(2)}, u32[]{:S(2)}) collective-permute-start(bf16[128,256]{0,1:T(8,128)(2,1)} %bitcast.11), channel_id=1, source_target_pairs={{0,4},{4,8},{8,12},{12,16},{16,20},{20,24},{24,28},{1,5},{5,9},{9,... | collective-permute-start | bytes 196616 | tf_op jit(solution)/shard_map/ppermute | solution.py:19
  71.7 2.0 convolution_convert_fusion.2
  73.7 5.8 %convolution_convert_fusion = bf16[512,384]{0,1:T(8,128)(2,1)} fusion(bf16[512,4096]{0,1:T(8,128)(2,1)} %bitcast.122, bf16[4096,384]{1,0:T(8,128)(2,1)} %param.19), kind=kOutput, calls=%fused_computation.33 | convolution fusion | flops 1610809344 | bytes 7733248 | tf_op jit(solution)/shard_map/dot_general | solution.py:172
  79.8 4.9 %convolution_convert_fusion.3 = bf16[512,256]{1,0:T(8,128)(2,1)} fusion(bf16[512,4096]{0,1:T(8,128)(2,1)} %bitcast.123, bf16[4096,256]{1,0:T(8,128)(2,1)} %param.23), kind=kOutput, calls=%fused_computation.36 | convolution fusion | flops 1073872896 | bytes 6553600 | tf_op jit(solution)/shard_map/dot_general | solution.py:172
  84.8 0.9 pad_maximum_fusion
  85.7 1.7 fusion.23
  87.4 2.3 fusion.24
  89.8 2.7 fusion.40
  92.5 5.6 %fusion.52 = f32[512,4096]{1,0:T(8,128)} fusion(bf16[512,384]{0,1:T(8,128)(2,1)S(1)} %bitcast.134, bf16[384,4096]{1,0:T(8,128)(2,1)S(1)} %copy-done), kind=kOutput, calls=%fused_computation.68 | convolution fusion | flops 1610612736 | bytes 11927552 | tf_op jit(solution)/shard_map/dot_general | solution.py:178
  98.1 9.4 %all-gather.7.cloned.1.call-done = bf16[4096,256]{1,0:T(8,128)(2,1)} async-done(((bf16[512,256]{1,0:T(8,128)(2,1)}), bf16[4096,256]{1,0:T(8,128)(2,1)}) %all-gather.7.cloned.1.call-update) | async-done | bytes 2097168 | tf_op jit(solution)/shard_map/all_gather | solution.py:126
  107.5 49.8 %all-gather.5.cloned.1.call-done = bf16[4096,256]{1,0:T(8,128)(2,1)} async-done(((bf16[512,256]{1,0:T(8,128)(2,1)}), bf16[4096,256]{1,0:T(8,128)(2,1)}) %all-gather.5.cloned.1.call-update) | async-done | bytes 2097168 | tf_op jit(solution)/shard_map/all_gather | solution.py:125
  157.2 89.2 %conditional.1 = (f32[4,2,512]{2,1,0:T(2,128)}, f32[4,2,512,64]{2,3,1,0:T(8,128)}) conditional(s32[]{:T(128)} %convert_element_type.55, () %tuple.34, (s32[512]{0:T(512)S(1)}, bf16[512,256]{1,0:T(8,128)(2,1)S(1)}, bf16[4096,256]{1,0:T(8,128)(2,1)}, bf16[4096,256]{1,0:T(8,128)(2,1)}, s32[]{:T(128)}, /*index=5*/s32[]{:T(128)}) %tuple.80), branch_computations={%region_3.4_spmd, %region_4.9_spmd.clone} | conditional | flops 859970048 | bytes 132364824 | solution.py:127
  158.7 4.1 %copy.44 = bf16[4096,256]{0,1:T(8,128)(2,1)} copy(bf16[4096,256]{1,0:T(8,128)(2,1)} %get-tuple-element.257) | data formatting | bytes 4194304 | tf_op jit(solution)/shard_map
  162.8 2.9 copy.43
  166.4 1.1 broadcast_in_dim.105
  167.5 79.0 %while.37 = (s32[]{:T(128)}, f32[4,2,512]{2,1,0:T(2,128)S(1)}, f32[4,2,512]{2,1,0:T(2,128)}, f32[4,2,512,64]{2,3,1,0:T(8,128)}, s32[]{:T(128)}, /*index=5*/s32[]...) while((s32[]{:T(128)}, f32[4,2,512]{2,1,0:T(2,128)S(1)}, ...), condition=%wide.region_8.8_spmd, body=%wide.region_5.7_spmd.sunk | while | flops 859969536 | bytes 122368224 | solution.py:109
  168.1 2.7 fusion.82
  170.9 4.9 %fusion.83 = f32[4,2,128]{2,1,0:T(2,128)S(1)} fusion(f32[4,2,128,4096]{3,2,1,0:T(8,128)S(1)} %get-tuple-element.364, f32[4,2,128]{2,1,0:T(2,128)S(1)} %get-tuple-element.365, pred[4096]{0:T(1024)(128)(4,1)S(1)} %iota_compare_fusion.2), kind=kLoop, calls=%fused_computation.4.clone.1 | loop fusion | flops 20970496 | bytes 16789504 | tf_op jit(solution)/shard_map/cond/branch_1_fun/while/body/while/body/eval_jaxpr/reduce_sum | solution.py:93
  175.8 0.8 copy-done.2
  176.6 1.3 add_dynamic-update-slice_fusion.2
  177.9 9.3 %fusion.84 = f32[4,2,512,64]{2,3,1,0:T(8,128)} fusion(f32[4,2,512,64]{2,3,1,0:T(8,128)} %get-tuple-element.384, s32[]{:T(128)S(6)} %select_n.128, bf16[4096,4,64]{0,2,1:T(8,128)(2,1)} %get-tuple-element.402, f32[4,2,128,4096]{3,2,1,0:T(8,128)} %copy-done.2, f32[4,2,128]{2,1,0:T(2,128)S(1)} %get-tuple-element.365, ...), kind=kOutput, calls=%fused_computation.9.clone.1 | convolution fusion | flops 557973504 | bytes 19410948 | tf_op jit(solution)/shard_map/cond/branch_1_fun/while/body/while/body/eval_jaxpr/hmqk,khd->hmqd/dot_general | solution.py:94
  187.9 2.7 fusion.82
  190.7 4.9 %fusion.83 = f32[4,2,128]{2,1,0:T(2,128)S(1)} fusion(f32[4,2,128,4096]{3,2,1,0:T(8,128)S(1)} %get-tuple-element.364, f32[4,2,128]{2,1,0:T(2,128)S(1)} %get-tuple-element.365, pred[4096]{0:T(1024)(128)(4,1)S(1)} %iota_compare_fusion.2), kind=kLoop, calls=%fused_computation.4.clone.1 | loop fusion | flops 20970496 | bytes 16789504 | tf_op jit(solution)/shard_map/cond/branch_1_fun/while/body/while/body/eval_jaxpr/reduce_sum | solution.py:93
  195.5 0.8 copy-done.2
  196.4 1.2 add_dynamic-update-slice_fusion.2
  197.6 9.3 %fusion.84 = f32[4,2,512,64]{2,3,1,0:T(8,128)} fusion(f32[4,2,512,64]{2,3,1,0:T(8,128)} %get-tuple-element.384, s32[]{:T(128)S(6)} %select_n.128, bf16[4096,4,64]{0,2,1:T(8,128)(2,1)} %get-tuple-element.402, f32[4,2,128,4096]{3,2,1,0:T(8,128)} %copy-done.2, f32[4,2,128]{2,1,0:T(2,128)S(1)} %get-tuple-element.365, ...), kind=kOutput, calls=%fused_computation.9.clone.1 | convolution fusion | flops 557973504 | bytes 19410948 | tf_op jit(solution)/shard_map/cond/branch_1_fun/while/body/while/body/eval_jaxpr/hmqk,khd->hmqd/dot_general | solution.py:94
  207.6 2.7 fusion.82
  210.4 4.9 %fusion.83 = f32[4,2,128]{2,1,0:T(2,128)S(1)} fusion(f32[4,2,128,4096]{3,2,1,0:T(8,128)S(1)} %get-tuple-element.364, f32[4,2,128]{2,1,0:T(2,128)S(1)} %get-tuple-element.365, pred[4096]{0:T(1024)(128)(4,1)S(1)} %iota_compare_fusion.2), kind=kLoop, calls=%fused_computation.4.clone.1 | loop fusion | flops 20970496 | bytes 16789504 | tf_op jit(solution)/shard_map/cond/branch_1_fun/while/body/while/body/eval_jaxpr/reduce_sum | solution.py:93
  215.2 0.8 copy-done.2
  216.1 1.3 add_dynamic-update-slice_fusion.2
  217.4 9.3 %fusion.84 = f32[4,2,512,64]{2,3,1,0:T(8,128)} fusion(f32[4,2,512,64]{2,3,1,0:T(8,128)} %get-tuple-element.384, s32[]{:T(128)S(6)} %select_n.128, bf16[4096,4,64]{0,2,1:T(8,128)(2,1)} %get-tuple-element.402, f32[4,2,128,4096]{3,2,1,0:T(8,128)} %copy-done.2, f32[4,2,128]{2,1,0:T(2,128)S(1)} %get-tuple-element.365, ...), kind=kOutput, calls=%fused_computation.9.clone.1 | convolution fusion | flops 557973504 | bytes 19410948 | tf_op jit(solution)/shard_map/cond/branch_1_fun/while/body/while/body/eval_jaxpr/hmqk,khd->hmqd/dot_general | solution.py:94
  227.3 2.7 fusion.82
  230.1 4.9 %fusion.83 = f32[4,2,128]{2,1,0:T(2,128)S(1)} fusion(f32[4,2,128,4096]{3,2,1,0:T(8,128)S(1)} %get-tuple-element.364, f32[4,2,128]{2,1,0:T(2,128)S(1)} %get-tuple-element.365, pred[4096]{0:T(1024)(128)(4,1)S(1)} %iota_compare_fusion.2), kind=kLoop, calls=%fused_computation.4.clone.1 | loop fusion | flops 20970496 | bytes 16789504 | tf_op jit(solution)/shard_map/cond/branch_1_fun/while/body/while/body/eval_jaxpr/reduce_sum | solution.py:93
  235.0 0.8 copy-done.2
  235.8 1.3 add_dynamic-update-slice_fusion.2
  237.1 9.3 %fusion.84 = f32[4,2,512,64]{2,3,1,0:T(8,128)} fusion(f32[4,2,512,64]{2,3,1,0:T(8,128)} %get-tuple-element.384, s32[]{:T(128)S(6)} %select_n.128, bf16[4096,4,64]{0,2,1:T(8,128)(2,1)} %get-tuple-element.402, f32[4,2,128,4096]{3,2,1,0:T(8,128)} %copy-done.2, f32[4,2,128]{2,1,0:T(2,128)S(1)} %get-tuple-element.365, ...), kind=kOutput, calls=%fused_computation.9.clone.1 | convolution fusion | flops 557973504 | bytes 19410948 | tf_op jit(solution)/shard_map/cond/branch_1_fun/while/body/while/body/eval_jaxpr/hmqk,khd->hmqd/dot_general | solution.py:94
  246.4 0.9 compare_select_fusion
  247.3 1.4 broadcast_divide_fusion
  249.1 6.8 %add_convert_fusion = bf16[512,4096]{1,0:T(8,128)(2,1)} fusion(f32[512,4096]{1,0:T(8,128)} %fusion.52, bf16[512,256]{0,1:T(8,128)(2,1)S(1)} %bitcast.129, bf16[256,4096]{1,0:T(8,128)(2,1)S(1)} %copy-done.4), kind=kOutput, calls=%fused_computation.23 | convolution fusion | flops 1077936128 | bytes 14942208 | tf_op jit(solution)/shard_map/dot_general | solution.py:180
  256.0 43.2 %reduce-scatter.2.cloned.1.call-done = bf16[128,4096]{1,0:T(8,128)(2,1)} async-done(((bf16[512,4096]{1,0:T(8,128)(2,1)}), bf16[128,4096]{1,0:T(8,128)(2,1)}) %reduce-scatter.2.cloned.1.call-update) | async-done | bytes 1048592 | tf_op jit(solution)/shard_map/reduce_scatter | solution.py:179
  (76 shorter events, 7.0 us)
Async XLA Ops:
  6.5 85.9 %copy-start = (bf16[384,4096]{1,0:T(8,128)(2,1)S(1)}, bf16[384,4096]{1,0:T(8,128)(2,1)}, u32[]{:S(2)}) copy-start(bf16[384,4096]{1,0:T(8,128)(2,1)} %param.28) | copy-start | bytes 9437188
  6.5 39.6 %all-gather.9.cloned.1.call-start = ((), (), s32[]{:S(2)}) async-start(), calls=%async_computation.4 | async-start | bytes 5242880 | tf_op jit(solution)/shard_map/all_gather | solution.py:169
  7.3 100.2 %all-gather.7.cloned.1.call-start = ((), (), s32[]{:S(2)}) async-start(), calls=%async_computation.2 | async-start | bytes 2359296 | tf_op jit(solution)/shard_map/all_gather | solution.py:126
  52.3 5.6 %copy-start.15 = (f32[6]{0:T(128)S(1)}, f32[6]{0:T(128)}, u32[]{:S(2)}) copy-start(f32[6]{0:T(128)} %param.22) | copy-start | bytes 76
  57.2 100.0 %all-gather.5.cloned.1.call-start = ((), (), s32[]{:S(2)}) async-start(), calls=%async_computation.1 | async-start | bytes 2359296 | tf_op jit(solution)/shard_map/all_gather | solution.py:125
  58.0 4.5 %copy-start.3 = (bf16[512,4,1024]{0,2,1:T(8,128)(2,1)S(1)}, bf16[512,4,1024]{0,2,1:T(8,128)(2,1)}, u32[]{:S(2)}) copy-start(bf16[512,4,1024]{0,2,1:T(8,128)(2,1)} %copy.28) | copy-start | bytes 12582916
  58.0 4.5 %copy-start.14 = (bf16[4096,128]{1,0:T(8,128)(2,1)S(1)}, bf16[4096,128]{1,0:T(8,128)(2,1)}, u32[]{:S(2)}) copy-start(bf16[4096,128]{1,0:T(8,128)(2,1)} %param.20) | copy-start | bytes 3145732
  62.6 0.8 copy-start.5
  62.6 9.2 %copy-start.13 = (bf16[4096,256]{1,0:T(8,128)(2,1)S(1)}, bf16[4096,256]{1,0:T(8,128)(2,1)}, u32[]{:S(2)}) copy-start(bf16[4096,256]{1,0:T(8,128)(2,1)} %param.24) | copy-start | bytes 6291460
  63.4 0.6 copy-start.7
  65.3 19.5 %collective-permute-start.1 = (bf16[128,256]{0,1:T(8,128)(2,1)}, bf16[128,256]{0,1:T(8,128)(2,1)}, u32[]{:S(2)}, u32[]{:S(2)}) collective-permute-start(bf16[128,256]{0,1:T(8,128)(2,1)} %bitcast.13), channel_id=1, source_target_pairs={{4,0},{8,4},{12,8},{16,12},{20,16},{24,20},{28,24},{5,1},{9,5},{13... | collective-permute-start | bytes 196616 | tf_op jit(solution)/shard_map/ppermute | solution.py:22
  66.6 18.2 %collective-permute-start = (bf16[128,256]{0,1:T(8,128)(2,1)}, bf16[128,256]{0,1:T(8,128)(2,1)}, u32[]{:S(2)}, u32[]{:S(2)}) collective-permute-start(bf16[128,256]{0,1:T(8,128)(2,1)} %bitcast.11), channel_id=1, source_target_pairs={{0,4},{4,8},{8,12},{12,16},{16,20},{20,24},{24,28},{1,5},{5,9},{9,... | collective-permute-start | bytes 196616 | tf_op jit(solution)/shard_map/ppermute | solution.py:19
  79.5 219.7 %reduce-scatter.2.cloned.1.call-start = ((), (), s32[]{:S(2)}) async-start(), calls=%async_computation.3 | async-start | bytes 5242880 | tf_op jit(solution)/shard_map/reduce_scatter | solution.py:179
  79.8 5.0 %copy-start.6 = (bf16[512,128]{0,1:T(8,128)(2,1)S(1)}, bf16[512,128]{0,1:T(8,128)(2,1)}, u32[]{:S(2)}) copy-start(bf16[512,128]{0,1:T(8,128)(2,1)} %copy-done.5) | copy-start | bytes 393220
  79.8 5.0 %copy-start.8 = (bf16[512,128]{0,1:T(8,128)(2,1)S(1)}, bf16[512,128]{0,1:T(8,128)(2,1)}, u32[]{:S(2)}) copy-start(bf16[512,128]{0,1:T(8,128)(2,1)} %copy-done.7) | copy-start | bytes 393220
  79.8 5.9 %copy-start.9 = (bf16[512,384]{0,1:T(8,128)(2,1)S(1)}, bf16[512,384]{0,1:T(8,128)(2,1)}, u32[]{:S(2)}) copy-start(bf16[512,384]{0,1:T(8,128)(2,1)} %convolution_convert_fusion) | copy-start | bytes 1179652
  92.5 64.8 %copy-start.10 = (bf16[512,256]{1,0:T(8,128)(2,1)S(1)}, bf16[512,256]{1,0:T(8,128)(2,1)}, u32[]{:S(2)}) copy-start(bf16[512,256]{1,0:T(8,128)(2,1)} %convolution_convert_fusion.3) | copy-start | bytes 786436
  157.2 91.4 %copy-start.11 = (f32[4]{0:T(128)S(1)}, f32[4]{0:T(128)}, u32[]{:S(2)}) copy-start(f32[4]{0:T(128)} %param.26) | copy-start | bytes 52
  157.2 91.7 %copy-start.12 = (f32[64]{0:T(128)S(1)}, f32[64]{0:T(128)}, u32[]{:S(2)}) copy-start(f32[64]{0:T(128)} %param.27) | copy-start | bytes 772
  170.9 5.7 %copy-start.2 = (f32[4,2,128,4096]{3,2,1,0:T(8,128)}, f32[4,2,128,4096]{3,2,1,0:T(8,128)S(1)}, u32[]{:S(2)}) copy-start(f32[4,2,128,4096]{3,2,1,0:T(8,128)S(1)} %get-tuple-element.364) | copy-start | bytes 50331652 | tf_op jit(solution)/shard_map/cond/branch_1_fun/while
  190.6 5.7 %copy-start.2 = (f32[4,2,128,4096]{3,2,1,0:T(8,128)}, f32[4,2,128,4096]{3,2,1,0:T(8,128)S(1)}, u32[]{:S(2)}) copy-start(f32[4,2,128,4096]{3,2,1,0:T(8,128)S(1)} %get-tuple-element.364) | copy-start | bytes 50331652 | tf_op jit(solution)/shard_map/cond/branch_1_fun/while
  210.3 5.7 %copy-start.2 = (f32[4,2,128,4096]{3,2,1,0:T(8,128)}, f32[4,2,128,4096]{3,2,1,0:T(8,128)S(1)}, u32[]{:S(2)}) copy-start(f32[4,2,128,4096]{3,2,1,0:T(8,128)S(1)} %get-tuple-element.364) | copy-start | bytes 50331652 | tf_op jit(solution)/shard_map/cond/branch_1_fun/while
  230.1 5.7 %copy-start.2 = (f32[4,2,128,4096]{3,2,1,0:T(8,128)}, f32[4,2,128,4096]{3,2,1,0:T(8,128)S(1)}, u32[]{:S(2)}) copy-start(f32[4,2,128,4096]{3,2,1,0:T(8,128)S(1)} %get-tuple-element.364) | copy-start | bytes 50331652 | tf_op jit(solution)/shard_map/cond/branch_1_fun/while
  246.4 2.7 copy-start.4
  249.1 50.1 %copy-start.1 = (bf16[384,4096]{1,0:T(8,128)(2,1)S(1)}, bf16[384,4096]{1,0:T(8,128)(2,1)}, u32[]{:S(2)}) copy-start(bf16[384,4096]{1,0:T(8,128)(2,1)} %param.28) | copy-start | bytes 9437188
Sparse Core Ops, SparseCore 0:
  8.9 37.1 all-gather.8
  57.3 50.0 all-gather.6
  109.6 47.6 all-gather.4
  256.1 43.0 reduce-scatter.1
